TPU v7x, 32 devices: a whole 2x2x4 slice. The times are simulated.
32 devices in a mesh: sp: 16 (over z, y, x), tp: 2 (over core).
Axes of the slice: x: 2, y: 2, z: 4, core: 2. Of those that a mesh axis runs over, the one named last changes fastest.
Arguments:
- prompt: bfloat16 [1, 8192, 2048], P(None, 'sp', 'tp'), may hold values from -6 to 6
- new_token: bfloat16 [1, 2048], P(None, 'tp'), may hold values from -6 to 6
- w_query: bfloat16 [2048, 2048], P(None, 'tp'), may hold values from -0.125 to 0.125
- w_key: bfloat16 [2048, 2048], P(None, 'tp'), may hold values from -0.125 to 0.125
- w_value: bfloat16 [2048, 2048], P(None, 'tp'), may hold values from -0.125 to 0.125
- decay_rate: float32 [16], P('tp'), may hold values from 1e-05 to 0.06
- norm_gain: float32 [2048], P('tp'), may hold values from 0.1 to 1.9
Outputs:
- mixed: bfloat16 [1, 8192, 2048], P(None, 'sp', 'tp')
- cache: bfloat16 [1, 16, 128, 128], P(None, 'tp', 'sp')
- new_read: bfloat16 [1, 2048], P(None, 'tp')
All inputs are finite; a program needn't handle non-finite values.
Results may differ from a plain program's by a relative error of at most 0.0083.
Values may be sent and summed in bfloat16 or wider, within the bound.
A program may use at most 64 MiB of HBM per device.

v0:
```python
import jax
import jax.numpy as jnp
from jax import lax
from jax.sharding import PartitionSpec as P

HEAD = 128
rope_base = 10000.0
norm_floor = 1e-05


def rotate(tensor, positions):
    head_width = tensor.shape[-1]
    inverse = rope_base ** (-jnp.arange(0, head_width, 2, dtype=jnp.float32) / head_width)
    angles = positions.astype(jnp.float32)[:, None] * inverse[None, :]
    cosine = jnp.cos(angles)[:, None, :]
    sine_part = jnp.sin(angles)[:, None, :]
    first_half = tensor[..., : head_width // 2]
    second_half = tensor[..., head_width // 2 :]
    return jnp.concatenate(
        [
            first_half * cosine - second_half * sine_part,
            first_half * sine_part + second_half * cosine,
        ],
        axis=-1,
    )


def head_norm(output, gain):
    center = jnp.mean(output, axis=-1, keepdims=True)
    spread = jnp.mean(jnp.square(output - center), axis=-1, keepdims=True)
    return (output - center) * lax.rsqrt(spread + norm_floor) * gain


def decay_tables(log_gamma, block_size):
    offsets = jnp.arange(block_size, dtype=jnp.float32)
    gap_table = offsets[:, None] - offsets[None, :]
    within = jnp.where(
        gap_table[None] >= 0,
        jnp.exp(jnp.maximum(gap_table, 0.0)[None] * log_gamma[:, None, None]),
        0.0,
    )
    query_decay = jnp.exp((offsets[:, None] + 1.0) * log_gamma[None, :])
    key_decay = jnp.exp((block_size - 1.0 - offsets[:, None]) * log_gamma[None, :])
    return (within, query_decay, key_decay)


def per_device(prompt, new_token, w_query, w_key, w_value, decay_rate, norm_gain):
    sequences, block_size, feature_part = prompt.shape
    head_count = w_query.shape[1] // HEAD
    members = lax.axis_size("sp")
    device_rank = lax.axis_index("sp")
    prompt_rows = sequences * block_size
    token_rows = jnp.concatenate([prompt.reshape(prompt_rows, feature_part), new_token], axis=0)
    weight_list = (w_query, w_key, w_value)
    shard_piece = lax.all_gather(token_rows, "tp", axis=1, tiled=True)
    projected = tuple(
        (jnp.dot(shard_piece, weight, preferred_element_type=jnp.float32) for weight in weight_list)
    )
    full_shape = (sequences, block_size, head_count, HEAD)
    queries, key_rows, values = [
        tensor[:prompt_rows].astype(jnp.bfloat16).reshape(full_shape) for tensor in projected
    ]
    token_query, token_key, token_value = [
        tensor[prompt_rows:].astype(jnp.bfloat16).reshape(sequences, 1, head_count, HEAD)
        for tensor in projected
    ]
    positions = device_rank * block_size + jnp.arange(block_size, dtype=jnp.int32)
    scaled = (rotate(queries.astype(jnp.float32), positions) * HEAD ** (-0.5)).astype(jnp.bfloat16)
    turned = rotate(key_rows.astype(jnp.float32), positions).astype(jnp.bfloat16)
    log_gamma = -decay_rate
    within, query_decay, key_decay = decay_tables(log_gamma, block_size)
    weighted = (turned.astype(jnp.float32) * key_decay[None, :, :, None]).astype(jnp.bfloat16)
    local_state = jnp.einsum(
        "smhd,smhe->shde", weighted, values, preferred_element_type=jnp.float32
    )
    pieces = lax.all_to_all(local_state[None], "sp", split_axis=3, concat_axis=0, tiled=True)
    source_index = jnp.arange(members, dtype=jnp.float32)
    gap_table = source_index[:, None] - 1.0 - source_index[None, :]
    weights = jnp.where(
        gap_table[None] >= 0,
        jnp.exp(jnp.maximum(gap_table, 0.0)[None] * block_size * log_gamma[:, None, None]),
        0.0,
    )
    prefix = jnp.einsum("hji,ishre->jshre", weights, pieces, precision=lax.Precision.HIGHEST)
    tail_all = jnp.exp((members - 1.0 - source_index)[None, :] * block_size * log_gamma[:, None])
    final_rows = jnp.einsum("hi,ishre->shre", tail_all, pieces, precision=lax.Precision.HIGHEST)
    incoming = lax.all_to_all(
        prefix.astype(jnp.bfloat16), "sp", split_axis=0, concat_axis=3, tiled=True
    ).astype(prefix.dtype)[0]
    scores = (
        jnp.einsum("snhd,smhd->shnm", scaled, turned, preferred_element_type=jnp.float32)
        * within[None]
    )
    inner_part = jnp.einsum(
        "shnm,smhe->snhe", scores.astype(jnp.bfloat16), values, preferred_element_type=jnp.float32
    )
    carried = (
        jnp.einsum(
            "snhd,shde->snhe",
            scaled,
            incoming.astype(jnp.bfloat16),
            preferred_element_type=jnp.float32,
        )
        * query_decay[None, :, :, None]
    )
    gain = norm_gain.reshape(head_count, HEAD)
    mixed = (
        head_norm(inner_part + carried, gain)
        .astype(jnp.bfloat16)
        .reshape(sequences, block_size, head_count * HEAD)
    )
    cache = final_rows.astype(jnp.bfloat16)
    token_positions = jnp.full((1,), block_size * members, jnp.int32)
    token_scaled = (
        rotate(token_query.astype(jnp.float32), token_positions) * HEAD ** (-0.5)
    ).astype(jnp.bfloat16)[:, 0]
    token_turned = rotate(token_key.astype(jnp.float32), token_positions).astype(jnp.bfloat16)[:, 0]
    row_count = final_rows.shape[2]
    query_rows = lax.dynamic_slice_in_dim(
        token_scaled, device_rank * row_count, row_count, 2
    ).astype(jnp.float32)
    partial_value = jnp.einsum(
        "shr,shre->she", query_rows, final_rows, precision=lax.Precision.HIGHEST
    )
    read_sum = lax.psum(partial_value, "sp")
    own_score = jnp.sum(
        token_scaled.astype(jnp.float32) * token_turned.astype(jnp.float32), axis=-1, keepdims=True
    )
    read_out = jnp.exp(log_gamma)[None, :, None] * read_sum + own_score * token_value[:, 0].astype(
        jnp.float32
    )
    new_read = head_norm(read_out, gain).astype(jnp.bfloat16).reshape(sequences, head_count * HEAD)
    return (mixed, cache, new_read)


def solution(mesh):
    in_specs = (
        P(None, "sp", "tp"),
        P(None, "tp"),
        P(None, "tp"),
        P(None, "tp"),
        P(None, "tp"),
        P("tp"),
        P("tp"),
    )
    out_specs = (P(None, "sp", "tp"), P(None, "tp", "sp", None), P(None, "tp"))
    return jax.shard_map(
        per_device, mesh=mesh, in_specs=in_specs, out_specs=out_specs, check_vma=False
    )
```

profile of v0, /device:TPU:0, one launch (start us, length us, event | category | flops | bytes accessed | tf_op | source)
XLA Modules:
  0.0 131.3 jit_solution(5846563984525811698)
XLA Ops:
  7.2 0.0 all-gather.2.cloned.1.call-start
  7.2 2.3 %pad_maximum_fusion = bf16[513,1024]{1,0:T(8,128)(2,1)} fusion(bf16[1,1024]{1,0:T(2,128)(2,1)} %param.8, bf16[512,1024]{1,0:T(8,128)(2,1)} %bitcast.117), kind=kLoop, calls=%fused_computation.26 | loop fusion | flops 2101248 | bytes 2101248 | tf_op jit(solution)/shard_map/concatenate | solution.py:53
  9.6 0.1 multiply_sine_fusion.1
  9.7 0.3 fusion.16
  10.0 1.2 fusion.15
  11.1 0.1 fusion.34
  11.2 0.1 multiply_exponential_fusion.2
  11.3 0.1 maximum_multiply_fusion.1
  11.3 0.1 multiply_exponential_fusion.1
  11.4 1.0 multiply_cosine_fusion
  12.4 10.7 %all-gather.2.cloned.1.call-done = bf16[513,2048]{1,0:T(8,128)(2,1)} async-done(((bf16[513,1024]{1,0:T(8,128)(2,1)}), bf16[513,2048]{1,0:T(8,128)(2,1)}) %all-gather.2.cloned.1.call-update) | async-done | bytes 2101264 | tf_op jit(solution)/shard_map/all_gather | solution.py:55
  23.1 5.3 %convolution_convert_fusion = bf16[513,1024]{1,0:T(8,128)(2,1)S(1)} fusion(bf16[513,2048]{1,0:T(8,128)(2,1)} %all-gather.2.cloned.1.call-done, bf16[2048,1024]{1,0:T(8,128)(2,1)} %param.10), kind=kOutput, calls=%fused_computation.20 | convolution fusion | flops 2152203264 | bytes 7346176 | tf_op jit(solution)/shard_map/dot_general | solution.py:57
  28.5 0.2 convert_bitcast_fusion
  28.7 1.3 %copy-done.7 = bf16[513,2048]{1,0:T(8,128)(2,1)S(1)} copy-done((bf16[513,2048]{1,0:T(8,128)(2,1)S(1)}, bf16[513,2048]{1,0:T(8,128)(2,1)}, u32[]{:S(2)}) %copy-start.7) | copy-done | bytes 2101272
  30.0 2.4 %convolution_convert_fusion.1 = bf16[513,1024]{1,0:T(8,128)(2,1)S(1)} fusion(bf16[513,2048]{1,0:T(8,128)(2,1)S(1)} %copy-done.7, bf16[2048,1024]{1,0:T(8,128)(2,1)S(1)} %copy-done.5), kind=kOutput, calls=%fused_computation.21 | convolution fusion | flops 2152203264 | bytes 7346176 | tf_op jit(solution)/shard_map/dot_general | solution.py:57
  32.5 0.2 convert_bitcast_fusion.1
  32.7 0.5 copy.71
  33.2 0.5 copy.70
  33.7 1.3 %fusion.49 = (f32[1,512,8,64]{3,2,1,0:T(8,128)S(1)}, f32[1,512,8,64]{3,2,1,0:T(8,128)S(1)}, f32[1,512,8,64]{3,2,1,0:T(8,128)S(1)}, f32[1,512,8,64]{3,2,1,0:T(8,128)S(1)}) fusion(f32[1,512,8,128]{3,2,1,0:T(8,128)S(1)} %bitcast.112, f32[1,512,8,128]{3,2,1,0:T(8,128)S(1)} %bitcast.113), kind=kLoop, calls=%fused_computation.104 | loop fusion | bytes 8388608 | tf_op jit(solution)/shard_map/slice | solution.py:17
  35.0 2.8 %fusion.10 = (bf16[512,8,64]{2,0,1:T(8,128)(2,1)S(1)}, bf16[512,8,64]{2,0,1:T(8,128)(2,1)S(1)}, f32[512,8,64]{2,0,1:T(8,128)S(1)}, f32[512,8,64]{2,0,1:T(8,128)}) fusion(f32[1,512,8,64]{3,2,1,0:T(8,128)S(1)} %get-tuple-element.22, f32[1,512,8,64]{3,2,1,0:T(8,128)S(1)} %get-tuple-element.21, f32[512,64]{1,0:T(8,128)S(1)} %get-tuple-element.32, ...), kind=kLoop, calls=%fused_computation.27 | loop fusion | flops 3670016 | bytes 7602176 | tf_op jit(solution)/shard_map/concatenate | solution.py:19
  37.9 2.4 %convolution_convert_fusion.2 = bf16[513,1024]{1,0:T(8,128)(2,1)S(1)} fusion(bf16[513,2048]{1,0:T(8,128)(2,1)S(1)} %copy-done.7, bf16[2048,1024]{1,0:T(8,128)(2,1)S(1)} %copy-done.6), kind=kOutput, calls=%fused_computation.22 | convolution fusion | flops 2152203264 | bytes 7346176 | tf_op jit(solution)/shard_map/dot_general | solution.py:57
  40.3 2.6 %convolution_bitcast_fusion = f32[1,1,8,128,128]{4,3,2,1,0:T(8,128)S(1)} fusion(f32[512,8]{0,1:T(8,128)S(1)} %get-tuple-element.37, bf16[512,8,64]{2,0,1:T(8,128)(2,1)S(1)} %get-tuple-element.18, bf16[512,8,64]{2,0,1:T(8,128)(2,1)S(1)} %get-tuple-element.17, bf16[513,1024]{1,0:T(8,128)(2,1)S(1)} %convolution_convert_fusion.2), kind=kOutput, calls=%fused_computation.23 | convolution fusion | flops 137363456 | bytes 3686400 | tf_op jit(solution)/shard_map/smhd,smhe->shde/dot_general | solution.py:73
  43.0 1.1 copy.49
  44.1 6.8 %all-to-all-start = ((f32[1,1,8,128,128]{4,2,1,0,3:T(8,128)}), f32[1,1,8,128,128]{4,2,1,0,3:T(8,128)S(1)}, u32[]{:S(2)}, u32[]{:S(2)}) async-start(f32[1,1,8,128,128]{4,2,1,0,3:T(8,128)} %copy.49), calls=%async_computation | async-start | bytes 1048576 | tf_op jit(solution)/shard_map/all_to_all | solution.py:76
  50.9 0.1 fusion.40
  51.0 0.1 fusion.35
  51.0 0.1 dynamic-slice_bitcast_fusion
  51.1 0.2 multiply_reduce_fusion.2
  51.3 3.2 %fusion.7 = bf16[512,8,128]{2,0,1:T(8,128)(2,1)} fusion(f32[512,8,64]{2,0,1:T(8,128)S(1)} %get-tuple-element.25, f32[512,8,64]{2,0,1:T(8,128)} %get-tuple-element.26), kind=kLoop, calls=%fused_computation.8 | loop fusion | flops 1572864 | bytes 3145728 | tf_op jit(solution)/shard_map/convert_element_type | solution.py:68
  54.5 0.7 slice_convert_fusion
  55.2 7.4 %fusion = f32[8,128,512]{2,1,0:T(8,128)} fusion(f32[8]{0:T(128)S(1)} %get-tuple-element.36, f32[512,512]{1,0:T(8,128)} %fusion.15, pred[512,512]{1,0:T(8,128)(4,1)S(1)} %fusion.16, bf16[512,8,128]{2,0,1:T(8,128)(2,1)} %fusion.7, bf16[512,8,64]{2,0,1:T(8,128)(2,1)} %copy-done.2, bf16[512,8,64]{2,0,1:T(8,128)(2,1)} %copy-done.1, bf16[513,1024]{1,0:T(8,128)(2,1)} %copy-done.4), kind=kOutput, calls=%fused_computation.1 | convolution fusion | flops 1084227584 | bytes 7602208 | tf_op jit(solution)/shard_map/shnm,smhe->snhe/dot_general | solution.py:94
  62.6 3.8 %all-to-all-done = f32[1,1,8,128,128]{4,2,1,0,3:T(8,128)S(1)} async-done(((f32[1,1,8,128,128]{4,2,1,0,3:T(8,128)}), f32[1,1,8,128,128]{4,2,1,0,3:T(8,128)S(1)}, u32[]{:S(2)}, u32[]{:S(2)}) %all-to-all-start) | async-done | bytes 524320 | tf_op jit(solution)/shard_map/all_to_all | solution.py:76
  66.4 0.7 fusion.19
  67.1 0.9 fusion.9
  68.0 0.8 copy.52
  68.7 0.1 fusion.38
  68.9 39.2 %psum.7 = f32[1,8,128]{2,1,0:T(8,128)S(1)} all-reduce(f32[1,8,128]{2,1,0:T(8,128)S(1)} %bitcast.127), channel_id=1, replica_groups=mesh['sp'=16,'tp'=2] {'sp'}, use_global_device_ids=true, to_apply=%region_2.3 | all-reduce | flops 1024 | bytes 8192 | tf_op jit(solution)/shard_map/psum | solution.py:125
  108.1 0.2 fusion.48
  108.3 3.5 %all-to-all-start.1 = ((bf16[16,1,8,8,128]{4,3,2,1,0:T(8,128)(2,1)}), bf16[16,1,8,8,128]{4,3,2,1,0:T(8,128)(2,1)S(1)}, u32[]{:S(2)}, u32[]{:S(2)}) async-start(bf16[16,1,8,8,128]{4,3,2,1,0:T(8,128)(2,1)} %copy.52), calls=%async_computation.1 | async-start | bytes 524288 | tf_op jit(solution)/shard_map/all_to_all | solution.py:87
  111.8 0.2 multiply_reduce_fusion.1
  112.0 0.1 fusion.42
  112.1 0.6 copy.114
  112.7 0.6 convert_bitcast_fusion.2
  113.3 7.0 %all-to-all-done.1 = bf16[16,1,8,8,128]{4,3,2,1,0:T(8,128)(2,1)S(1)} async-done(((bf16[16,1,8,8,128]{4,3,2,1,0:T(8,128)(2,1)}), bf16[16,1,8,8,128]{4,3,2,1,0:T(8,128)(2,1)S(1)}, u32[]{:S(2)}, u32[]{:S(2)}) %all-to-all-start.1) | async-done | bytes 262176 | tf_op jit(solution)/shard_map/all_to_all | solution.py:87
  120.3 2.1 %fusion.51 = (f32[512,8]{0,1:T(8,128)S(1)}, f32[1,512,8,128]{1,3,2,0:T(8,128)S(1)}) fusion(f32[512,8]{0,1:T(8,128)S(1)} %get-tuple-element.38, bf16[512,8,128]{2,0,1:T(8,128)(2,1)S(1)} %copy-done, bf16[16,1,8,8,128]{4,3,2,1,0:T(8,128)(2,1)S(1)} %all-to-all-done.1, f32[8,128,512]{2,1,0:T(8,128)} %fusion), kind=kOutput, calls=%fused_computation.106 | convolution fusion | flops 135786496 | bytes 5537792 | tf_op jit(solution)/shard_map/snhd,shde->snhe/dot_general | solution.py:98
  122.4 0.3 multiply_reduce_fusion
  122.8 0.4 multiply_convert_fusion.2
  123.1 1.3 %copy.55 = bf16[1,512,1024]{2,1,0:T(8,128)(2,1)} copy(bf16[1,512,1024]{1,2,0:T(8,128)(2,1)S(1)} %bitcast.116) | data formatting | bytes 2097152
  (30 shorter events, 0.1 us)
Async XLA Ops:
  7.2 15.9 %all-gather.2.cloned.1.call-start = ((), (), s32[]{:S(2)}) async-start(), calls=%async_computation.2 | async-start | bytes 3194880 | tf_op jit(solution)/shard_map/all_gather | solution.py:55
  7.2 3.9 %copy-start.8 = (f32[8]{0:T(128)S(1)}, f32[8]{0:T(128)}, u32[]{:S(2)}) copy-start(f32[8]{0:T(128)} %param.12) | copy-start | bytes 100
  23.1 5.6 %copy-start.5 = (bf16[2048,1024]{1,0:T(8,128)(2,1)S(1)}, bf16[2048,1024]{1,0:T(8,128)(2,1)}, u32[]{:S(2)}) copy-start(bf16[2048,1024]{1,0:T(8,128)(2,1)} %param.9) | copy-start | bytes 12582916
  28.4 1.6 %copy-start.7 = (bf16[513,2048]{1,0:T(8,128)(2,1)S(1)}, bf16[513,2048]{1,0:T(8,128)(2,1)}, u32[]{:S(2)}) copy-start(bf16[513,2048]{1,0:T(8,128)(2,1)} %all-gather.2.cloned.1.call-done) | copy-start | bytes 6303748
  35.0 2.8 %copy-start.6 = (bf16[2048,1024]{1,0:T(8,128)(2,1)S(1)}, bf16[2048,1024]{1,0:T(8,128)(2,1)}, u32[]{:S(2)}) copy-start(bf16[2048,1024]{1,0:T(8,128)(2,1)} %param.11) | copy-start | bytes 12582916
  37.9 2.4 %copy-start.1 = (bf16[512,8,64]{2,0,1:T(8,128)(2,1)}, bf16[512,8,64]{2,0,1:T(8,128)(2,1)S(1)}, u32[]{:S(2)}) copy-start(bf16[512,8,64]{2,0,1:T(8,128)(2,1)S(1)} %get-tuple-element.17) | copy-start | bytes 1572868
  37.9 2.4 %copy-start.2 = (bf16[512,8,64]{2,0,1:T(8,128)(2,1)}, bf16[512,8,64]{2,0,1:T(8,128)(2,1)S(1)}, u32[]{:S(2)}) copy-start(bf16[512,8,64]{2,0,1:T(8,128)(2,1)S(1)} %get-tuple-element.18) | copy-start | bytes 1572868
  40.3 2.7 %copy-start.4 = (bf16[513,1024]{1,0:T(8,128)(2,1)}, bf16[513,1024]{1,0:T(8,128)(2,1)S(1)}, u32[]{:S(2)}) copy-start(bf16[513,1024]{1,0:T(8,128)(2,1)S(1)} %convolution_convert_fusion.2) | copy-start | bytes 3151876
  44.1 22.3 %all-to-all-start = ((f32[1,1,8,128,128]{4,2,1,0,3:T(8,128)}), f32[1,1,8,128,128]{4,2,1,0,3:T(8,128)S(1)}, u32[]{:S(2)}, u32[]{:S(2)}) async-start(f32[1,1,8,128,128]{4,2,1,0,3:T(8,128)} %copy.49), calls=%async_computation | async-start | bytes 1048576 | tf_op jit(solution)/shard_map/all_to_all | solution.py:76
  62.6 49.4 %copy-start.3 = (f32[1024]{0:T(1024)S(1)}, f32[1024]{0:T(1024)}, u32[]{:S(2)}) copy-start(f32[1024]{0:T(1024)} %param.13) | copy-start | bytes 12292
  62.6 57.7 %copy-start = (bf16[512,8,128]{2,0,1:T(8,128)(2,1)S(1)}, bf16[512,8,128]{2,0,1:T(8,128)(2,1)}, u32[]{:S(2)}) copy-start(bf16[512,8,128]{2,0,1:T(8,128)(2,1)} %fusion.7) | copy-start | bytes 3145732
  108.3 12.0 %all-to-all-start.1 = ((bf16[16,1,8,8,128]{4,3,2,1,0:T(8,128)(2,1)}), bf16[16,1,8,8,128]{4,3,2,1,0:T(8,128)(2,1)S(1)}, u32[]{:S(2)}, u32[]{:S(2)}) async-start(bf16[16,1,8,8,128]{4,3,2,1,0:T(8,128)(2,1)} %copy.52), calls=%async_computation.1 | async-start | bytes 524288 | tf_op jit(solution)/shard_map/all_to_all | solution.py:87
Sparse Core Ops, SparseCore 0:
  9.7 13.3 all-gather.1
where the time goes:
time: 132 us; the launch traced here: 131 us
  blocking collectives  39.2 us (30%)
  matrix products  24.1 us (18%)
  waiting for transfers between devices  21.4 us (16%)
  other arithmetic  14.4 us (11%)
  between operations  14.3 us (11%)
  starting transfers between devices  10.4 us (8%)
  local copies, waits for them, and re-layouts  7.52 us (6%)
    psum x1, blocking collectives, per_device(): read_sum = lax.psum(partial_value, 'sp')  39.2 us
    all_gather x1, waiting for transfers between devices, per_device(): shard_piece = lax.all_gather(token_rows, 'tp', axis=1, tiled=True)  10.7 us
    dot_general x3, matrix products, per_device(): jnp.dot(shard_piece, weight, preferred_element_type=jnp.float32)  10.2 us
    dot_general x1, matrix products, per_device(): jnp.einsum('shnm,smhe->snhe', scores.astype(jnp.bfloat16), values, prefer...  7.39 us
    all_to_all x1, waiting for transfers between devices, per_device(): lax.all_to_all(prefix.astype(jnp.bfloat16), 'sp', split_axis=0, concat_ax...  6.98 us
    all_to_all x1, starting transfers between devices, per_device(): lax.all_to_all(local_state[None], 'sp', split_axis=3, concat_axis=0, tile...  6.79 us
    unnamed x22, local copies, waits for them, and re-layouts  4.22 us
    all_to_all x1, waiting for transfers between devices, per_device(): lax.all_to_all(local_state[None], 'sp', split_axis=3, concat_axis=0, tile...  3.77 us
  transfers between devices with their start and end apart: 3, of which 3 were waited for; matrix products, arithmetic and copies ran while one was open for 12% of the time, Pallas kernels for 0%

commit v1 on v0

--- a/solution.py
+++ b/solution.py
@@ -6,6 +6,13 @@
 HEAD = 128
 rope_base = 10000.0
 norm_floor = 1e-05
+
+
+def exchange_blocks(value, mesh_axis, split, join):
+    size = lax.axis_size(mesh_axis)
+    shards = jnp.stack(jnp.split(value, size, axis=split), axis=0)
+    shards = lax.all_to_all(shards, mesh_axis, split_axis=0, concat_axis=0)
+    return jnp.concatenate(shards, axis=join)
 
 
 def rotate(tensor, positions):
@@ -84,9 +91,7 @@
     prefix = jnp.einsum("hji,ishre->jshre", weights, pieces, precision=lax.Precision.HIGHEST)
     tail_all = jnp.exp((members - 1.0 - source_index)[None, :] * block_size * log_gamma[:, None])
     final_rows = jnp.einsum("hi,ishre->shre", tail_all, pieces, precision=lax.Precision.HIGHEST)
-    incoming = lax.all_to_all(
-        prefix.astype(jnp.bfloat16), "sp", split_axis=0, concat_axis=3, tiled=True
-    ).astype(prefix.dtype)[0]
+    incoming = exchange_blocks(prefix.astype(jnp.bfloat16), "sp", 0, 3).astype(prefix.dtype)[0]
     scores = (
         jnp.einsum("snhd,smhd->shnm", scaled, turned, preferred_element_type=jnp.float32)
         * within[None]

time: 132 us -> 141 us (1.068)
  local copies, waits for them, and re-layouts: 7.52 us -> 16.9 us
    unnamed x22 -> x37, local copies, waits for them, and re-layouts: 4.22 us -> 13.3 us
  transfers between devices with their start and end apart: 3 -> 3, of which waited for: 3 -> 3; matrix products, arithmetic and copies ran while one was open for 12% -> 11% of each run, Pallas kernels for 0% -> 0%
where the time goes in v1:
time: 141 us
  blocking collectives  39.2 us (28%)
  matrix products  24.1 us (17%)
  waiting for transfers between devices  21.4 us (15%)
  local copies, waits for them, and re-layouts  16.9 us (12%)
  other arithmetic  14.4 us (10%)
  between operations  14.3 us (10%)
  starting transfers between devices  10.4 us (7%)
    psum x1, blocking collectives, per_device(): read_sum = lax.psum(partial_value, 'sp')  39.2 us
    unnamed x37, local copies, waits for them, and re-layouts  13.3 us
    all_gather x1, waiting for transfers between devices, per_device(): shard_piece = lax.all_gather(token_rows, 'tp', axis=1, tiled=True)  10.6 us
    dot_general x3, matrix products, per_device(): jnp.dot(shard_piece, weight, preferred_element_type=jnp.float32)  10.2 us
    dot_general x1, matrix products, per_device(): jnp.einsum('shnm,smhe->snhe', scores.astype(jnp.bfloat16), values, prefer...  7.4 us
    all_to_all x1, waiting for transfers between devices, exchange_blocks(): shards = lax.all_to_all(shards, mesh_axis, split_axis=0, concat_axis=0)  6.98 us
    all_to_all x1, starting transfers between devices, per_device(): lax.all_to_all(local_state[None], 'sp', split_axis=3, concat_axis=0, tile...  6.8 us
    all_to_all x1, waiting for transfers between devices, per_device(): lax.all_to_all(local_state[None], 'sp', split_axis=3, concat_axis=0, tile...  3.76 us
  transfers between devices with their start and end apart: 3, of which 3 were waited for; matrix products, arithmetic and copies ran while one was open for 11% of the time, Pallas kernels for 0%

profile of v1, /device:TPU:0, one launch (start us, length us, event | category | flops | bytes accessed | tf_op | source)
XLA Modules:
  0.0 140.7 jit_solution(18393202517669038599)
XLA Ops:
  7.2 2.3 %pad_maximum_fusion = bf16[513,1024]{1,0:T(8,128)(2,1)} fusion(bf16[1,1024]{1,0:T(2,128)(2,1)} %param.8, bf16[512,1024]{1,0:T(8,128)(2,1)} %bitcast.149), kind=kLoop, calls=%fused_computation.26 | loop fusion | flops 2101248 | bytes 2101248 | tf_op jit(solution)/shard_map/concatenate | solution.py:60
  9.7 0.3 fusion.16
  9.9 1.2 fusion.15
  11.4 1.0 multiply_cosine_fusion
  12.4 10.6 %all-gather.2.cloned.1.call-done = bf16[513,2048]{1,0:T(8,128)(2,1)} async-done(((bf16[513,1024]{1,0:T(8,128)(2,1)}), bf16[513,2048]{1,0:T(8,128)(2,1)}) %all-gather.2.cloned.1.call-update) | async-done | bytes 2101264 | tf_op jit(solution)/shard_map/all_gather | solution.py:62
  23.1 5.3 %convolution_convert_fusion = bf16[513,1024]{1,0:T(8,128)(2,1)S(1)} fusion(bf16[513,2048]{1,0:T(8,128)(2,1)} %all-gather.2.cloned.1.call-done, bf16[2048,1024]{1,0:T(8,128)(2,1)} %param.10), kind=kOutput, calls=%fused_computation.20 | convolution fusion | flops 2152203264 | bytes 7346176 | tf_op jit(solution)/shard_map/dot_general | solution.py:64
  28.7 1.3 copy-done.7
  30.0 2.4 %convolution_convert_fusion.1 = bf16[513,1024]{1,0:T(8,128)(2,1)S(1)} fusion(bf16[513,2048]{1,0:T(8,128)(2,1)S(1)} %copy-done.7, bf16[2048,1024]{1,0:T(8,128)(2,1)S(1)} %copy-done.5), kind=kOutput, calls=%fused_computation.21 | convolution fusion | flops 2152203264 | bytes 7346176 | tf_op jit(solution)/shard_map/dot_general | solution.py:64
  32.7 0.5 copy.370
  33.2 0.5 copy.369
  33.6 1.3 fusion.49
  35.0 2.8 %fusion.10 = (bf16[512,8,64]{2,0,1:T(8,128)(2,1)S(1)}, bf16[512,8,64]{2,0,1:T(8,128)(2,1)S(1)}, f32[512,8,64]{2,0,1:T(8,128)S(1)}, f32[512,8,64]{2,0,1:T(8,128)}) fusion(f32[1,512,8,64]{3,2,1,0:T(8,128)S(1)} %get-tuple-element.67, f32[1,512,8,64]{3,2,1,0:T(8,128)S(1)} %get-tuple-element.66, f32[512,64]{1,0:T(8,128)S(1)} %get-tuple-element.93, ...), kind=kLoop, calls=%fused_computation.27 | loop fusion | flops 3670016 | bytes 7602176 | tf_op jit(solution)/shard_map/concatenate | solution.py:26
  37.8 2.4 %convolution_convert_fusion.2 = bf16[513,1024]{1,0:T(8,128)(2,1)S(1)} fusion(bf16[513,2048]{1,0:T(8,128)(2,1)S(1)} %copy-done.7, bf16[2048,1024]{1,0:T(8,128)(2,1)S(1)} %copy-done.6), kind=kOutput, calls=%fused_computation.22 | convolution fusion | flops 2152203264 | bytes 7346176 | tf_op jit(solution)/shard_map/dot_general | solution.py:64
  40.3 2.6 %convolution_bitcast_fusion = f32[1,1,8,128,128]{4,3,2,1,0:T(8,128)S(1)} fusion(f32[512,8]{0,1:T(8,128)S(1)} %get-tuple-element.98, bf16[512,8,64]{2,0,1:T(8,128)(2,1)S(1)} %get-tuple-element.63, bf16[512,8,64]{2,0,1:T(8,128)(2,1)S(1)} %get-tuple-element.62, bf16[513,1024]{1,0:T(8,128)(2,1)S(1)} %convolution_convert_fusion.2), kind=kOutput, calls=%fused_computation.23 | convolution fusion | flops 137363456 | bytes 3686400 | tf_op jit(solution)/shard_map/smhd,smhe->shde/dot_general | solution.py:80
  42.9 1.1 copy.333
  44.1 6.8 %all-to-all-start = ((f32[1,1,8,128,128]{4,2,1,0,3:T(8,128)}), f32[1,1,8,128,128]{4,2,1,0,3:T(8,128)S(1)}, u32[]{:S(2)}, u32[]{:S(2)}) async-start(f32[1,1,8,128,128]{4,2,1,0,3:T(8,128)} %copy.333), calls=%async_computation | async-start | bytes 1048576 | tf_op jit(solution)/shard_map/all_to_all | solution.py:83
  51.3 3.2 %fusion.7 = bf16[512,8,128]{2,0,1:T(8,128)(2,1)} fusion(f32[512,8,64]{2,0,1:T(8,128)S(1)} %get-tuple-element.70, f32[512,8,64]{2,0,1:T(8,128)} %get-tuple-element.71), kind=kLoop, calls=%fused_computation.8 | loop fusion | flops 1572864 | bytes 3145728 | tf_op jit(solution)/shard_map/convert_element_type | solution.py:75
  54.5 0.7 slice_convert_fusion
  55.2 7.4 %fusion = f32[8,128,512]{2,1,0:T(8,128)} fusion(f32[8]{0:T(128)S(1)} %get-tuple-element.97, f32[512,512]{1,0:T(8,128)} %fusion.15, pred[512,512]{1,0:T(8,128)(4,1)S(1)} %fusion.16, bf16[512,8,128]{2,0,1:T(8,128)(2,1)} %fusion.7, bf16[512,8,64]{2,0,1:T(8,128)(2,1)} %copy-done.2, bf16[512,8,64]{2,0,1:T(8,128)(2,1)} %copy-done.1, bf16[513,1024]{1,0:T(8,128)(2,1)} %copy-done.4), kind=kOutput, calls=%fused_computation.1 | convolution fusion | flops 1084227584 | bytes 7602208 | tf_op jit(solution)/shard_map/shnm,smhe->snhe/dot_general | solution.py:99
  62.6 3.8 %all-to-all-done = f32[1,1,8,128,128]{4,2,1,0,3:T(8,128)S(1)} async-done(((f32[1,1,8,128,128]{4,2,1,0,3:T(8,128)}), f32[1,1,8,128,128]{4,2,1,0,3:T(8,128)S(1)}, u32[]{:S(2)}, u32[]{:S(2)}) %all-to-all-start) | async-done | bytes 524320 | tf_op jit(solution)/shard_map/all_to_all | solution.py:83
  66.3 0.7 fusion.19
  67.2 39.2 %psum.7 = f32[1,8,128]{2,1,0:T(8,128)S(1)} all-reduce(f32[1,8,128]{2,1,0:T(8,128)S(1)} %bitcast.159), channel_id=1, replica_groups=mesh['sp'=16,'tp'=2] {'sp'}, use_global_device_ids=true, to_apply=%region_2.3 | all-reduce | flops 1024 | bytes 8192 | tf_op jit(solution)/shard_map/psum | solution.py:130
  106.6 0.9 fusion.9
  107.5 0.5 fusion.51
  108.1 0.6 constant_dynamic-update-slice_fusion.15
  108.7 0.6 constant_dynamic-update-slice_fusion.14
  109.3 0.6 constant_dynamic-update-slice_fusion.13
  109.9 0.6 constant_dynamic-update-slice_fusion.12
  110.5 0.6 constant_dynamic-update-slice_fusion.11
  111.1 0.6 constant_dynamic-update-slice_fusion.10
  111.7 0.6 constant_dynamic-update-slice_fusion.9
  112.3 0.6 constant_dynamic-update-slice_fusion.8
  112.9 0.6 constant_dynamic-update-slice_fusion.7
  113.5 0.6 constant_dynamic-update-slice_fusion.6
  114.1 0.6 constant_dynamic-update-slice_fusion.5
  114.7 0.6 constant_dynamic-update-slice_fusion.4
  115.3 0.6 constant_dynamic-update-slice_fusion.3
  115.9 0.6 constant_dynamic-update-slice_fusion.2
  116.5 0.6 constant_dynamic-update-slice_fusion.1
  117.1 0.6 constant_dynamic-update-slice_fusion
  117.7 3.5 %all-to-all-start.1 = ((bf16[16,1,1,8,8,128]{5,4,3,2,1,0:T(8,128)(2,1)}), bf16[16,1,1,8,8,128]{5,4,3,2,1,0:T(8,128)(2,1)S(1)}, u32[]{:S(2)}, u32[]{:S(2)}) async-start(bf16[16,1,1,8,8,128]{5,4,3,2,1,0:T(8,128)(2,1)} %constant_dynamic-update-slice_fusion), calls=%async_computation.1 | async-start | bytes 524288 | tf_op jit(solution)/shard_map/all_to_all | solution.py:14
  121.5 0.6 copy.429
  122.1 0.6 convert_bitcast_fusion.2
  122.7 7.0 %all-to-all-done.1 = bf16[16,1,1,8,8,128]{5,4,3,2,1,0:T(8,128)(2,1)S(1)} async-done(((bf16[16,1,1,8,8,128]{5,4,3,2,1,0:T(8,128)(2,1)}), bf16[16,1,1,8,8,128]{5,4,3,2,1,0:T(8,128)(2,1)S(1)}, u32[]{:S(2)}, u32[]{:S(2)}) %all-to-all-start.1) | async-done | bytes 262176 | tf_op jit(solution)/shard_map/all_to_all | solution.py:14
  129.7 2.1 %fusion.52 = (f32[512,8]{0,1:T(8,128)S(1)}, f32[1,512,8,128]{1,3,2,0:T(8,128)S(1)}) fusion(f32[512,8]{0,1:T(8,128)S(1)} %get-tuple-element.99, bf16[512,8,128]{2,0,1:T(8,128)(2,1)S(1)} %copy-done, f32[8,128,512]{2,1,0:T(8,128)} %fusion, bf16[16,1,1,8,8,128]{5,4,3,2,1,0:T(8,128)(2,1)S(1)} %all-to-all-done.1), kind=kOutput, calls=%fused_computation.123 | convolution fusion | flops 135786496 | bytes 5537792 | tf_op jit(solution)/shard_map/snhd,shde->snhe/dot_general | solution.py:103
  131.9 0.3 multiply_reduce_fusion
  132.2 0.4 multiply_convert_fusion.2
  132.5 1.3 copy.338
  (46 shorter events, 2.0 us)
Async XLA Ops:
  7.2 15.9 %all-gather.2.cloned.1.call-start = ((), (), s32[]{:S(2)}) async-start(), calls=%async_computation.2 | async-start | bytes 3194880 | tf_op jit(solution)/shard_map/all_gather | solution.py:62
  7.2 3.9 %copy-start.8 = (f32[8]{0:T(128)S(1)}, f32[8]{0:T(128)}, u32[]{:S(2)}) copy-start(f32[8]{0:T(128)} %param.12) | copy-start | bytes 100
  23.0 5.6 %copy-start.5 = (bf16[2048,1024]{1,0:T(8,128)(2,1)S(1)}, bf16[2048,1024]{1,0:T(8,128)(2,1)}, u32[]{:S(2)}) copy-start(bf16[2048,1024]{1,0:T(8,128)(2,1)} %param.9) | copy-start | bytes 12582916
  28.4 1.6 %copy-start.7 = (bf16[513,2048]{1,0:T(8,128)(2,1)S(1)}, bf16[513,2048]{1,0:T(8,128)(2,1)}, u32[]{:S(2)}) copy-start(bf16[513,2048]{1,0:T(8,128)(2,1)} %all-gather.2.cloned.1.call-done) | copy-start | bytes 6303748
  35.0 2.8 %copy-start.6 = (bf16[2048,1024]{1,0:T(8,128)(2,1)S(1)}, bf16[2048,1024]{1,0:T(8,128)(2,1)}, u32[]{:S(2)}) copy-start(bf16[2048,1024]{1,0:T(8,128)(2,1)} %param.11) | copy-start | bytes 12582916
  37.8 2.4 %copy-start.1 = (bf16[512,8,64]{2,0,1:T(8,128)(2,1)}, bf16[512,8,64]{2,0,1:T(8,128)(2,1)S(1)}, u32[]{:S(2)}) copy-start(bf16[512,8,64]{2,0,1:T(8,128)(2,1)S(1)} %get-tuple-element.62) | copy-start | bytes 1572868
  37.8 2.4 %copy-start.2 = (bf16[512,8,64]{2,0,1:T(8,128)(2,1)}, bf16[512,8,64]{2,0,1:T(8,128)(2,1)S(1)}, u32[]{:S(2)}) copy-start(bf16[512,8,64]{2,0,1:T(8,128)(2,1)S(1)} %get-tuple-element.63) | copy-start | bytes 1572868
  40.2 2.7 %copy-start.4 = (bf16[513,1024]{1,0:T(8,128)(2,1)}, bf16[513,1024]{1,0:T(8,128)(2,1)S(1)}, u32[]{:S(2)}) copy-start(bf16[513,1024]{1,0:T(8,128)(2,1)S(1)} %convolution_convert_fusion.2) | copy-start | bytes 3151876
  44.1 22.3 %all-to-all-start = ((f32[1,1,8,128,128]{4,2,1,0,3:T(8,128)}), f32[1,1,8,128,128]{4,2,1,0,3:T(8,128)S(1)}, u32[]{:S(2)}, u32[]{:S(2)}) async-start(f32[1,1,8,128,128]{4,2,1,0,3:T(8,128)} %copy.333), calls=%async_computation | async-start | bytes 1048576 | tf_op jit(solution)/shard_map/all_to_all | solution.py:83
  62.6 58.9 %copy-start.3 = (f32[1024]{0:T(1024)S(1)}, f32[1024]{0:T(1024)}, u32[]{:S(2)}) copy-start(f32[1024]{0:T(1024)} %param.13) | copy-start | bytes 12292
  62.6 67.1 %copy-start = (bf16[512,8,128]{2,0,1:T(8,128)(2,1)S(1)}, bf16[512,8,128]{2,0,1:T(8,128)(2,1)}, u32[]{:S(2)}) copy-start(bf16[512,8,128]{2,0,1:T(8,128)(2,1)} %fusion.7) | copy-start | bytes 3145732
  117.7 12.0 %all-to-all-start.1 = ((bf16[16,1,1,8,8,128]{5,4,3,2,1,0:T(8,128)(2,1)}), bf16[16,1,1,8,8,128]{5,4,3,2,1,0:T(8,128)(2,1)S(1)}, u32[]{:S(2)}, u32[]{:S(2)}) async-start(bf16[16,1,1,8,8,128]{5,4,3,2,1,0:T(8,128)(2,1)} %constant_dynamic-update-slice_fusion), calls=%async_computation.1 | async-start | bytes 524288 | tf_op jit(solution)/shard_map/all_to_all | solution.py:14
Sparse Core Ops, SparseCore 0:
  9.7 13.3 all-gather.1
